TPU v7x, 512 devices: a whole 4x4x16 slice. The times are simulated.
512 devices in a mesh: sp: 64 (over z, y), tp: 8 (over x, core).
Axes of the slice: x: 4, y: 4, z: 16, core: 2. Of those that a mesh axis runs over, the one named last changes fastest.
Arguments:
- tokens: bfloat16 [49152, 2048], P(('sp', 'tp')), may hold values from -6 to 6
- input_gain: float32 [2048], replicated, may hold values from 0.1 to 1.9
- branch_value: bfloat16 [2048, 1024], P('sp', 'tp'), may hold values from -0.125 to 0.125
- branch_gate: bfloat16 [2048, 1024], P('sp', 'tp'), may hold values from -0.125 to 0.125
- query_weight: bfloat16 [2048, 1024], P('sp', 'tp'), may hold values from -0.125 to 0.125
- key_weight: bfloat16 [2048, 1024], P('sp', 'tp'), may hold values from -0.125 to 0.125
- value_weight: bfloat16 [2048, 1024], P('sp', 'tp'), may hold values from -0.125 to 0.125
- swish_weight: bfloat16 [2048, 1024], P('sp', 'tp'), may hold values from -0.125 to 0.125
- kernel_taps: float32 [31, 1024], P(None, 'tp'), may hold values from -8 to 8
- channel_gain: float32 [1024], P('tp'), may hold values from 0.1 to 1.9
- decay_logs: float32 [16, 49152], P('tp', 'sp'), may hold values from -1.5 to 0
- start_state: float32 [2, 16, 64, 64], P(None, 'tp')
- head_gain: float32 [1024], P('tp'), may hold values from 0.1 to 1.9
- output_conv: bfloat16 [1024, 2048], P('tp', 'sp'), may hold values from -0.125 to 0.125
- output_heads: bfloat16 [1024, 2048], P('tp', 'sp'), may hold values from -0.125 to 0.125
Outputs:
- mixed: bfloat16 [49152, 2048], P(('sp', 'tp'))
All inputs are finite; a program needn't handle non-finite values.
Results may differ from a plain program's by a relative error of at most 0.018.
Values may be sent and summed in bfloat16 or wider, within the bound.
No kernel may reach another device: no remote copies, remote signals or barrier semaphores. Data moves between devices by JAX's collectives and lax.ppermute only.
A program may use at most 64 MiB of HBM per device.

v0:
```python
import jax
import jax.numpy as jnp
from jax import lax
from jax.sharding import Mesh
from jax.sharding import PartitionSpec as P

DC = 1024
HD = 64
BLOCK = 256
SP = ("sp_0", "sp_1")
SP_TP = ("sp_0", "sp_1", "tp")
EPSILON = 1e-06


def sent_together(arrays, axis, dim, along):
    ends, at = ([], 0)
    for a in arrays[:-1]:
        at += a.shape[along]
        ends.append(at)
    both = jnp.concatenate(arrays, axis=along)
    return tuple(jnp.split(lax.all_gather(both, axis, axis=dim, tiled=True), ends, axis=along))


def with_halo(x, sides, width):
    for axis, dim in sides:
        count, length = (lax.axis_size(axis), x.shape[dim])
        up = [(i, (i + 1) % count) for i in range(count - 1)]
        down = [(j, i) for i, j in up]
        last = lax.slice_in_dim(x, length - width, length, axis=dim)
        first = lax.slice_in_dim(x, 0, width, axis=dim)
        before = lax.ppermute(last, axis, up)
        after = lax.ppermute(first, axis, down)
        x = jnp.concatenate([before, x, after], axis=dim)
    return x


def copy_for_each(x, axis):
    count = lax.axis_size(axis)
    return lax.all_to_all(jnp.broadcast_to(x[None], (count, *x.shape)), axis, 0, 0, tiled=True)


def over_copies(x, axis):
    everything = copy_for_each(x, axis)
    return jnp.sum(everything, axis=0)


def together(arrays, axis):
    ends = [0]
    for a in arrays:
        ends.append(ends[-1] + a.size)
    subtotal = over_copies(jnp.concatenate([a.ravel() for a in arrays]), axis)
    return tuple((subtotal[b:e].reshape(a.shape) for a, b, e in zip(arrays, ends, ends[1:])))


def filled_with(x, identity):
    return jax.tree.map(
        lambda part, zero: jnp.zeros_like(part) + jnp.asarray(zero, part.dtype), x, identity
    )


def all_in_one(x, axis):
    leaves = jax.tree.leaves(x)
    order = sorted(range(len(leaves)), key=lambda k: -leaves[k].size)
    width = (1, *leaves[order[0]].shape)[-1]
    lines = [
        jnp.pad(leaves[k].reshape(-1), (0, -leaves[k].size % width)).reshape(-1, width)
        for k in order
    ]
    both, at, found = (lax.all_gather(jnp.concatenate(lines), axis), 0, {})
    for k, line in zip(order, lines):
        section = both[:, at : at + len(line)].reshape(len(both), -1)
        found[k] = section[:, : leaves[k].size].reshape(-1, *leaves[k].shape)
        at += len(line)
    numbers = iter(range(len(leaves)))
    return jax.tree.map(lambda _: found[next(numbers)], x)


def prefix_by_axis(x, axes, combine, identity, reverse):
    before = start = filled_with(x, identity)
    subtotal = x
    for axis in reversed(axes):
        count, position = (lax.axis_size(axis), lax.axis_index(axis))
        pieces = all_in_one(
            jax.tree.map(
                lambda part, kind: part.astype(kind), subtotal, (jnp.bfloat16, jnp.bfloat16)
            ),
            axis,
        )
        inside, subtotal = (start, start)
        for k in reversed(range(count)) if reverse else range(count):
            passed = k > position if reverse else k < position
            subtotal = combine(
                subtotal, jax.tree.map(lambda part, own: part[k].astype(own.dtype), pieces, x)
            )
            inside = jax.tree.map(lambda new, old: jnp.where(passed, new, old), subtotal, inside)
        before = combine(inside, before)
    return before


def rows_first(arrays, axis, dims):
    turned = [jnp.moveaxis(a, dim, 0) for a, dim in zip(arrays, dims)]
    both = jnp.concatenate([t.reshape(len(t), -1) for t in turned], axis=1)
    out, at, gathered = (lax.all_gather(both, axis, axis=0, tiled=True), 0, [])
    for t, dim in zip(turned, dims):
        section = out[:, at : at + t[0].size].reshape(-1, *t.shape[1:])
        gathered.append(jnp.moveaxis(section, 0, dim))
        at += t[0].size
    return tuple(gathered)


def split_up(x, dim, count):
    shape = x.shape
    pieces = x.reshape(*shape[:dim], count, shape[dim] // count, *shape[dim + 1 :])
    return jnp.moveaxis(pieces, dim, 0)


def sum_at_owner(x, axis, dim):
    pieces = split_up(x, dim, lax.axis_size(axis))
    arrived = lax.all_to_all(pieces, axis, split_axis=0, concat_axis=0, tiled=True)
    return arrived.astype(jnp.float32).sum(axis=0)


def block_states(scaled_keys, values_block, running):
    closing = running[:, :, -1:]
    totals = jnp.exp(closing[:, :, 0])
    toward_end = jnp.exp(closing - running).transpose(0, 2, 1)[:, :, :, None]
    from_start = jnp.exp(running).transpose(0, 2, 1)[:, :, :, None]
    forward = jnp.einsum("nshd,nshe->nhde", scaled_keys * toward_end, values_block)
    backward = jnp.einsum("nshd,nshe->nhde", scaled_keys * from_start, values_block)
    return (totals, forward, backward)


def block_outputs(queries, scaled_keys, values_block, running, forward_in, backward_in):
    length = queries.shape[1]
    scores = jnp.einsum("nthd,nshd->nhts", queries, scaled_keys)
    distance = jnp.abs(running[:, :, :, None] - running[:, :, None, :])
    weights = jnp.exp(-distance) + jnp.eye(length, dtype=jnp.float32)
    within = jnp.einsum("nhts,nshe->nthe", scores * weights, values_block)
    from_start = jnp.exp(running).transpose(0, 2, 1)[:, :, :, None]
    toward_end = jnp.exp(running[:, :, -1:] - running).transpose(0, 2, 1)[:, :, :, None]
    earlier = jnp.einsum("nthd,nhde->nthe", queries, forward_in)
    after_part = jnp.einsum("nthd,nhde->nthe", queries, backward_in)
    return within + from_start * earlier + toward_end * after_part


def head_output(retained, gates_in, head_gain):
    row_count = retained.shape[0]
    centred = retained - jnp.mean(retained, axis=2, keepdims=True)
    scaled = centred * lax.rsqrt(jnp.mean(centred * centred, axis=2, keepdims=True) + EPSILON)
    flattened = scaled.reshape(row_count, -1) * head_gain[None, :]
    return (flattened * jax.nn.silu(gates_in.astype(jnp.float32))).astype(jnp.bfloat16)


def normalize(token_block, input_gain):
    widened = token_block.astype(jnp.float32)
    inverse = lax.rsqrt(jnp.mean(widened * widened, axis=1, keepdims=True) + EPSILON)
    return (widened * inverse * input_gain[None, :]).astype(jnp.bfloat16)


def input_mix(products):
    gated_rows = (products[0] * jax.nn.sigmoid(products[1])).astype(jnp.bfloat16)
    others = [member.astype(jnp.bfloat16) for member in products[2:]]
    return jnp.concatenate([gated_rows] + others, axis=1)


def combine_branches(earlier, latter):
    return (earlier[0] * latter[0], latter[0][:, None, None] * earlier[1] + latter[1])


def body(
    tokens,
    input_gain,
    branch_value,
    branch_gate,
    query_weight,
    key_weight,
    value_weight,
    swish_weight,
    kernel_taps,
    channel_gain,
    decay_logs,
    start_state,
    head_gain,
    output_conv,
    output_heads,
):
    projections = (branch_value, branch_gate, query_weight, key_weight, value_weight, swish_weight)
    full_column_count = sent_together(
        (
            projections[0],
            projections[1],
            projections[2],
            projections[3],
            projections[4],
            projections[5],
        ),
        SP,
        0,
        1,
    )
    normed = normalize(lax.all_gather(tokens, "tp", axis=0, tiled=True), input_gain)
    packed = input_mix(
        tuple(
            (
                jnp.dot(normed, weight, preferred_element_type=jnp.float32)
                for weight in full_column_count
            )
        )
    )
    value_width = branch_value.shape[1]
    head_width = query_weight.shape[1]
    row_count = packed.shape[0]
    gated_rows = packed[:, :value_width]
    queries_in = packed[:, value_width : value_width + head_width]
    keys_in = packed[:, value_width + head_width : value_width + 2 * head_width]
    values_in = packed[:, value_width + 2 * head_width : value_width + 3 * head_width]
    gates_in = packed[:, value_width + 3 * head_width :]
    half_width = kernel_taps.shape[0] // 2
    padded = with_halo(gated_rows, ((SP, 0),), half_width).astype(jnp.float32)
    convolved = jnp.zeros((row_count, value_width), jnp.float32)
    for offset in range(kernel_taps.shape[0]):
        convolved = convolved + kernel_taps[offset][None, :] * padded[offset : offset + row_count]
    moments = together((jnp.sum(convolved, axis=1), jnp.sum(convolved * convolved, axis=1)), "tp")
    average = (moments[0] / DC)[:, None]
    squares = (moments[1] / DC)[:, None]
    normalized = (convolved - average) * lax.rsqrt(squares - average * average + EPSILON)
    branch_out = jax.nn.silu(normalized * channel_gain[None, :]).astype(jnp.bfloat16)
    local_heads = head_width // HD
    blocks = row_count // BLOCK

    def split_heads(matrix):
        return matrix.astype(jnp.float32).reshape(blocks, BLOCK, local_heads, HD)

    query_blocks = split_heads(queries_in)
    key_blocks = split_heads(keys_in) * HD ** (-0.5)
    value_blocks = split_heads(values_in)
    running = jnp.cumsum(decay_logs.reshape(local_heads, blocks, BLOCK).transpose(1, 0, 2), axis=2)
    totals, forward, backward = block_states(key_blocks, value_blocks, running)
    forward_part = []
    forward_scale = []
    carried = jnp.zeros_like(forward[0])
    factor = jnp.ones_like(totals[0])
    for block_index in range(blocks):
        forward_part.append(carried)
        forward_scale.append(factor)
        carried = totals[block_index][:, None, None] * carried + forward[block_index]
        factor = factor * totals[block_index]
    device_forward = carried
    device_total = factor
    backward_part = [None] * blocks
    reverse_direction_scale = [None] * blocks
    carried = jnp.zeros_like(backward[0])
    factor = jnp.ones_like(totals[0])
    for block_index in reversed(range(blocks)):
        backward_part[block_index] = carried
        reverse_direction_scale[block_index] = factor
        carried = totals[block_index][:, None, None] * carried + backward[block_index]
        factor = factor * totals[block_index]
    identity = (jnp.ones_like(device_total), jnp.zeros_like(device_forward))
    before = prefix_by_axis((device_total, device_forward), SP, combine_branches, identity, False)
    after = prefix_by_axis((device_total, carried), SP, combine_branches, identity, True)
    enter_forward = before[1] + before[0][:, None, None] * start_state[0]
    enter_backward = after[1] + after[0][:, None, None] * start_state[1]
    forward_in = jnp.stack(
        [
            forward_scale[block_index][:, None, None] * enter_forward + forward_part[block_index]
            for block_index in range(blocks)
        ]
    )
    backward_in = jnp.stack(
        [
            reverse_direction_scale[block_index][:, None, None] * enter_backward
            + backward_part[block_index]
            for block_index in range(blocks)
        ]
    )
    retained = block_outputs(
        query_blocks, key_blocks, value_blocks, running, forward_in, backward_in
    )
    heads_out = head_output(retained.reshape(row_count, local_heads, HD), gates_in, head_gain)
    out_columns = rows_first((output_conv, output_heads), SP, (1, 1))
    combined = jnp.dot(branch_out, out_columns[0], preferred_element_type=jnp.float32)
    summed = sum_at_owner(
        (combined + jnp.dot(heads_out, out_columns[1], preferred_element_type=jnp.float32)).astype(
            jnp.bfloat16
        ),
        "tp",
        0,
    )
    return summed.astype(jnp.bfloat16)


def solution(mesh):
    split = Mesh(mesh.devices.reshape(16, 4, mesh.shape["tp"]), ("sp_0", "sp_1", "tp"))
    in_specs = (
        P(SP_TP, None),
        P(),
        P(SP, "tp"),
        P(SP, "tp"),
        P(SP, "tp"),
        P(SP, "tp"),
        P(SP, "tp"),
        P(SP, "tp"),
        P(None, "tp"),
        P("tp"),
        P("tp", SP),
        P(None, "tp", None, None),
        P("tp"),
        P("tp", SP),
        P("tp", SP),
    )
    out_specs = P(SP_TP, None)
    return jax.shard_map(body, mesh=split, in_specs=in_specs, out_specs=out_specs, check_vma=False)
```

profile of v0, /device:TPU:32, one launch (start us, length us, event | category | flops | bytes accessed | tf_op | source)
XLA Modules:
  0.0 487.4 jit_solution(7230470878673933972)
XLA Ops:
  14.4 1.8 reduce-window.6
  17.3 1.6 slice_bitcast_fusion.61
  18.9 1.6 slice_bitcast_fusion.62
  27.8 21.2 %all-gather.12.cloned.1.call-done = bf16[768,2048]{1,0:T(8,128)(2,1)} async-done(((bf16[96,2048]{1,0:T(8,128)(2,1)}), bf16[768,2048]{1,0:T(8,128)(2,1)}) %all-gather.12.cloned.1.call-update) | async-done | bytes 3145744 | tf_op jit(solution)/shard_map/all_gather | solution.py:201
  48.9 2.7 fusion
  52.6 143.0 %all-gather.14.cloned.1.call-done = bf16[2048,768]{1,0:T(8,128)(2,1)} async-done(((bf16[32,768]{1,0:T(8,128)(2,1)}), bf16[2048,768]{1,0:T(8,128)(2,1)}) %all-gather.14.cloned.1.call-update) | async-done | bytes 3145744 | tf_op jit(solution)/shard_map/all_gather | solution.py:21
  195.6 2.0 convolution_convert_fusion.3
  199.8 2.8 fusion.29
  202.7 1.9 copy.305
  204.6 2.0 reshape.1739
  206.6 2.0 broadcast_multiply_fusion.2
  215.8 1.5 copy.348
  217.3 1.5 copy.350
  218.9 1.5 copy.349
  222.0 12.1 %all-gather.4 = bf16[4,129,64]{1,2,0:T(8,128)(2,1)S(1)} all-gather(bf16[1,129,64]{1,2,0:T(8,128)(2,1)S(1)} %get-tuple-element.78), channel_id=2, replica_groups=mesh['sp_0'=16,'sp_1'=4,'tp'=8] {'sp_1'}, dimensions={0}, use_global_device_ids=true | all-gather | bytes 82560 | tf_op jit(solution)/shard_map/all_gather | solution.py:69
  236.0 12.0 %all-gather.6 = bf16[4,129,64]{1,2,0:T(8,128)(2,1)S(1)} all-gather(bf16[1,129,64]{1,2,0:T(8,128)(2,1)S(1)} %get-tuple-element.79), channel_id=4, replica_groups=mesh['sp_0'=16,'sp_1'=4,'tp'=8] {'sp_1'}, dimensions={0}, use_global_device_ids=true | all-gather | bytes 82560 | tf_op jit(solution)/shard_map/all_gather | solution.py:69
  263.7 29.0 %all-gather.7 = bf16[16,129,64]{1,2,0:T(8,128)(2,1)S(1)} all-gather(bf16[1,129,64]{1,2,0:T(8,128)(2,1)S(1)} %maximum_bitcast_fusion.1), channel_id=5, replica_groups=mesh['sp_0'=16,'sp_1'=4,'tp'=8] {'sp_0'}, dimensions={0}, use_global_device_ids=true | all-gather | bytes 280704 | tf_op jit(solution)/shard_map/all_gather | solution.py:69
  310.8 31.0 %all-gather.5 = bf16[16,129,64]{1,2,0:T(8,128)(2,1)S(1)} all-gather(bf16[1,129,64]{1,2,0:T(8,128)(2,1)S(1)} %maximum_bitcast_fusion), channel_id=3, replica_groups=mesh['sp_0'=16,'sp_1'=4,'tp'=8] {'sp_0'}, dimensions={0}, use_global_device_ids=true | all-gather | bytes 280704 | tf_op jit(solution)/shard_map/all_gather | solution.py:69
  345.6 2.7 convolution_convert_fusion.2
  348.3 1.9 reshape.1847
  350.2 1.9 copy.306
  363.9 2.0 fusion.41
  365.9 2.0 fusion.27
  368.8 1.9 collective-permute-start
  370.7 6.2 %collective-permute-start.1 = (bf16[15,128]{1,0:T(8,128)(2,1)}, bf16[15,128]{1,0:T(8,128)(2,1)}, u32[]{:S(2)}, u32[]{:S(2)}) collective-permute-start(bf16[15,128]{1,0:T(8,128)(2,1)} %get-tuple-element.69), channel_id=1, source_target_pairs={{8,0},{16,8},{24,16},{32,24},{40,32},{48,40},{56,48},{64,56},{72,6... | collective-permute-start | bytes 11528 | tf_op jit(solution)/shard_map/ppermute | solution.py:32
  411.4 1.5 fusion.160
  413.6 4.3 all-to-all-start
  420.8 2.6 all-to-all-done
  423.5 4.7 fusion.38
  428.2 7.7 %add_convert_fusion = bf16[768,2048]{1,0:T(8,128)(2,1)S(1)} fusion(f32[768,2048]{1,0:T(8,128)} %fusion.38, bf16[2048,256]{1,0:T(8,128)(2,1)} %all-gather.16.cloned.1.call-done, bf16[768,2048]{1,0:T(8,128)(2,1)} %copy-done.1, bf16[2048,768]{1,0:T(8,128)(2,1)} %all-gather.14.cloned.1.call-done, f32[768,128]{1,0:T(8,128)S(1)} %copy.379, ...), kind=kOutput, calls=%fused_computation.5 | convolution fusion | flops 809533440 | bytes 14811648 | tf_op jit(solution)/shard_map/dot_general | solution.py:284
  435.9 41.7 %all_to_all.11 = bf16[8,96,2048]{2,1,0:T(8,128)(2,1)} all-to-all(bf16[8,96,2048]{2,1,0:T(8,128)(2,1)S(1)} %bitcast.522), channel_id=1, replica_groups=mesh['sp_0'=16,'sp_1'=4,'tp'=8] {'tp'}, dimensions={0} | all-to-all | bytes 6291456 | tf_op jit(solution)/shard_map/all_to_all | solution.py:119
  477.6 3.3 reduce_sum.72
  (319 shorter events, 117.0 us)
Async XLA Ops:
  6.5 45.1 %copy-start.26 = (f32[2048]{0:T(1024)S(1)}, f32[2048]{0:T(1024)}, u32[]{:S(2)}) copy-start(f32[2048]{0:T(1024)} %param.16) | copy-start | bytes 24580
  6.5 42.4 %all-gather.12.cloned.1.call-start = ((), (), s32[]{:S(2)}) async-start(), calls=%async_computation.2 | async-start | bytes 3538944 | tf_op jit(solution)/shard_map/all_gather | solution.py:201
  7.3 188.3 %all-gather.14.cloned.1.call-start = ((), (), s32[]{:S(2)}) async-start(), calls=%async_computation.3 | async-start | bytes 3194880 | tf_op jit(solution)/shard_map/all_gather | solution.py:21
  12.2 411.3 %all-gather.16.cloned.1.call-start = ((), (), s32[]{:S(2)}) async-start(), calls=%async_computation.4 | async-start | bytes 1064960 | tf_op jit(solution)/shard_map/all_gather | solution.py:103
  21.6 30.9 %copy-start.32 = (f32[2]{0:T(128)}, f32[2]{0:T(128)S(1)}, u32[]{:S(2)}) copy-start(f32[2]{0:T(128)S(1)} %get-tuple-element.8) | copy-start | bytes 28
  52.6 313.3 %copy-start.1 = (bf16[768,2048]{1,0:T(8,128)(2,1)}, bf16[768,2048]{1,0:T(8,128)(2,1)S(1)}, u32[]{:S(2)}) copy-start(bf16[768,2048]{1,0:T(8,128)(2,1)S(1)} %fusion.2) | copy-start | bytes 9437188
  234.2 59.2 %copy-start.21 = (bf16[4,64]{1,0:T(4,128)(2,1)}, bf16[4,64]{1,0:T(4,128)(2,1)S(1)}, u32[]{:S(2)}) copy-start(bf16[4,64]{1,0:T(4,128)(2,1)S(1)} %slice_reduce_fusion.1) | copy-start | bytes 1540
  248.1 94.4 %copy-start.23 = (bf16[4,64]{1,0:T(4,128)(2,1)}, bf16[4,64]{1,0:T(4,128)(2,1)S(1)}, u32[]{:S(2)}) copy-start(bf16[4,64]{1,0:T(4,128)(2,1)S(1)} %slice_reduce_fusion) | copy-start | bytes 1540
  368.0 35.6 %copy-start.19 = (f32[1,128,64]{1,2,0:T(8,128)S(1)}, f32[1,128,64]{1,2,0:T(8,128)}, u32[]{:S(2)}) copy-start(f32[1,128,64]{1,2,0:T(8,128)} %get-tuple-element.45) | copy-start | bytes 98308
  368.0 35.7 %copy-start.24 = (bf16[4,64]{1,0:T(4,128)(2,1)S(1)}, bf16[4,64]{1,0:T(4,128)(2,1)}, u32[]{:S(2)}) copy-start(bf16[4,64]{1,0:T(4,128)(2,1)} %copy-done.23) | copy-start | bytes 1540
  368.0 35.7 %copy-start.43 = (f32[2]{0:T(128)S(1)}, f32[2]{0:T(128)}, u32[]{:S(2)}) copy-start(f32[2]{0:T(128)} %get-tuple-element.23) | copy-start | bytes 28
  368.0 35.8 %copy-start.22 = (bf16[4,64]{1,0:T(4,128)(2,1)S(1)}, bf16[4,64]{1,0:T(4,128)(2,1)}, u32[]{:S(2)}) copy-start(bf16[4,64]{1,0:T(4,128)(2,1)} %copy-done.21) | copy-start | bytes 1540
  368.0 35.8 %copy-start.42 = (f32[2]{0:T(128)S(1)}, f32[2]{0:T(128)}, u32[]{:S(2)}) copy-start(f32[2]{0:T(128)} %get-tuple-element.15) | copy-start | bytes 28
  368.0 35.8 %copy-start.11 = (f32[1,128,64]{2,1,0:T(8,128)S(1)}, f32[1,128,64]{2,1,0:T(8,128)}, u32[]{:S(2)}) copy-start(f32[1,128,64]{2,1,0:T(8,128)} %copy.339) | copy-start | bytes 98308
  368.0 35.8 %copy-start.12 = (f32[1,128,64]{2,1,0:T(8,128)S(1)}, f32[1,128,64]{2,1,0:T(8,128)}, u32[]{:S(2)}) copy-start(f32[1,128,64]{2,1,0:T(8,128)} %copy.341) | copy-start | bytes 98308
  368.0 35.8 %copy-start.13 = (f32[1,128,64]{2,1,0:T(8,128)S(1)}, f32[1,128,64]{2,1,0:T(8,128)}, u32[]{:S(2)}) copy-start(f32[1,128,64]{2,1,0:T(8,128)} %copy.340) | copy-start | bytes 98308
  368.0 35.8 %copy-start.14 = (f32[1,128,64]{2,1,0:T(8,128)S(1)}, f32[1,128,64]{2,1,0:T(8,128)}, u32[]{:S(2)}) copy-start(f32[1,128,64]{2,1,0:T(8,128)} %copy.342) | copy-start | bytes 98308
  368.1 35.8 %copy-start.29 = (f32[2]{0:T(128)S(1)}, f32[2]{0:T(128)}, u32[]{:S(2)}) copy-start(f32[2]{0:T(128)} %copy-done.28) | copy-start | bytes 28
  368.1 35.8 %copy-start.33 = (f32[2]{0:T(128)S(1)}, f32[2]{0:T(128)}, u32[]{:S(2)}) copy-start(f32[2]{0:T(128)} %copy-done.32) | copy-start | bytes 28
  368.1 35.8 %copy-start.35 = (f32[2]{0:T(128)S(1)}, f32[2]{0:T(128)}, u32[]{:S(2)}) copy-start(f32[2]{0:T(128)} %get-tuple-element.147) | copy-start | bytes 28
  368.1 35.8 %copy-start.36 = (f32[2]{0:T(128)S(1)}, f32[2]{0:T(128)}, u32[]{:S(2)}) copy-start(f32[2]{0:T(128)} %get-tuple-element.114) | copy-start | bytes 28
  368.1 35.8 %copy-start.37 = (f32[2]{0:T(128)S(1)}, f32[2]{0:T(128)}, u32[]{:S(2)}) copy-start(f32[2]{0:T(128)} %get-tuple-element.115) | copy-start | bytes 28
  368.1 35.8 %copy-start.38 = (f32[2]{0:T(128)S(1)}, f32[2]{0:T(128)}, u32[]{:S(2)}) copy-start(f32[2]{0:T(128)} %get-tuple-element.116) | copy-start | bytes 28
  368.1 35.8 %copy-start.39 = (f32[2]{0:T(128)S(1)}, f32[2]{0:T(128)}, u32[]{:S(2)}) copy-start(f32[2]{0:T(128)} %get-tuple-element.117) | copy-start | bytes 28
  368.1 35.8 %copy-start.40 = (f32[2]{0:T(128)S(1)}, f32[2]{0:T(128)}, u32[]{:S(2)}) copy-start(f32[2]{0:T(128)} %get-tuple-element.118) | copy-start | bytes 28
  368.1 37.0 %copy-start.7 = (f32[1,128,64]{2,1,0:T(8,128)S(1)}, f32[1,128,64]{2,1,0:T(8,128)}, u32[]{:S(2)}) copy-start(f32[1,128,64]{2,1,0:T(8,128)} %copy.370) | copy-start | bytes 98308
  368.1 37.0 %copy-start.8 = (f32[1,128,64]{2,1,0:T(8,128)S(1)}, f32[1,128,64]{2,1,0:T(8,128)}, u32[]{:S(2)}) copy-start(f32[1,128,64]{2,1,0:T(8,128)} %copy.372) | copy-start | bytes 98308
  368.2 37.0 %copy-start.9 = (f32[1,128,64]{2,1,0:T(8,128)S(1)}, f32[1,128,64]{2,1,0:T(8,128)}, u32[]{:S(2)}) copy-start(f32[1,128,64]{2,1,0:T(8,128)} %copy.371) | copy-start | bytes 98308
  368.2 37.0 %copy-start.10 = (f32[1,128,64]{2,1,0:T(8,128)S(1)}, f32[1,128,64]{2,1,0:T(8,128)}, u32[]{:S(2)}) copy-start(f32[1,128,64]{2,1,0:T(8,128)} %copy.373) | copy-start | bytes 98308
  368.8 41.5 %collective-permute-start = (bf16[15,128]{1,0:T(8,128)(2,1)}, bf16[15,128]{1,0:T(8,128)(2,1)}, u32[]{:S(2)}, u32[]{:S(2)}) collective-permute-start(bf16[15,128]{1,0:T(8,128)(2,1)} %get-tuple-element.68), channel_id=1, source_target_pairs={{0,8},{8,16},{16,24},{24,32},{32,40},{40,48},{48,56},{56,64},{64,7... | collective-permute-start | bytes 11528 | tf_op jit(solution)/shard_map/ppermute | solution.py:31
  370.7 39.6 %collective-permute-start.1 = (bf16[15,128]{1,0:T(8,128)(2,1)}, bf16[15,128]{1,0:T(8,128)(2,1)}, u32[]{:S(2)}, u32[]{:S(2)}) collective-permute-start(bf16[15,128]{1,0:T(8,128)(2,1)} %get-tuple-element.69), channel_id=1, source_target_pairs={{8,0},{16,8},{24,16},{32,24},{40,32},{48,40},{56,48},{64,56},{72,6... | collective-permute-start | bytes 11528 | tf_op jit(solution)/shard_map/ppermute | solution.py:32
  413.6 9.8 %all-to-all-start = ((f32[8,1,1536]{2,1,0:T(1,128)}), f32[8,1,1536]{2,1,0:T(1,128)S(1)}, u32[]{:S(2)}, u32[]{:S(2)}) async-start(f32[8,1,1536]{2,1,0:T(1,128)} %broadcast_in_dim.2), calls=%async_computation | async-start | bytes 98304 | tf_op jit(solution)/shard_map/all_to_all | solution.py:39
  (50 other events, 332.6 us)
Sparse Core Ops, SparseCore 0:
  9.5 39.4 all-gather.11
  51.9 143.6 all-gather.13
  198.5 133.8 all-gather.15
where the time goes:
time: 492 us; the launch traced here: 487 us
  waiting for transfers between devices  168 us (34%)
  blocking collectives  126 us (26%)
  local copies, waits for them, and re-layouts  107 us (22%)
  other arithmetic  31.9 us (6%)
  matrix products  28 us (6%)
  between operations  14.7 us (3%)
  starting transfers between devices  12.5 us (3%)
    all_gather x1, waiting for transfers between devices, sent_together(): lax.all_gather(both, axis, axis=dim, tiled=True)  143 us
    all_gather x4, blocking collectives, all_in_one(): both, at, found = (lax.all_gather(jnp.concatenate(lines), axis), 0, {})  84 us
    all_to_all x1, blocking collectives, sum_at_owner(): lax.all_to_all(pieces, axis, split_axis=0, concat_axis=0, tiled=True)  41.7 us
    convert_element_type x40, local copies, waits for them, and re-layouts, prefix_by_axis(): part[k].astype(own.dtype)  38.4 us
    all_gather x1, waiting for transfers between devices, body(): lax.all_gather(tokens, 'tp', axis=0, tiled=True)  21.2 us
    mul x16, local copies, waits for them, and re-layouts, combine_branches(): latter[0][:, None, None] * earlier[1] + latter[1]  20 us
    dot_general x5, matrix products, body(): jnp.dot(normed, weight, preferred_element_type=jnp.float32)  11.6 us
  transfers between devices with their start and end apart: 6, of which 3 were waited for; matrix products, arithmetic and copies ran while one was open for 31% of the time, Pallas kernels for 0%

commit v1 on v0

--- a/solution.py
+++ b/solution.py
@@ -198,7 +198,12 @@
         0,
         1,
     )
-    normed = normalize(lax.all_gather(tokens, "tp", axis=0, tiled=True), input_gain)
+    normed = normalize(
+        jnp.concatenate(
+            lax.all_to_all(jnp.stack([tokens] * lax.axis_size("tp")), "tp", 0, 0), axis=0
+        ),
+        input_gain,
+    )
     packed = input_mix(
         tuple(
             (

time: 492 us -> 458 us (0.931)
  waiting for transfers between devices: 168 us -> 127 us
    all_gather x1, waiting for transfers between devices: 143 us -> 98.5 us  [sent_together(): lax.all_gather(both, axis, axis=dim, tiled=True)]
    all_to_all x0 -> x1, waiting for transfers between devices: none -> 26.1 us  [body(): lax.all_to_all(jnp.stack([tokens] * lax.axis_size('tp')), 'tp', 0, 0)]
    all_gather x1 -> x0, waiting for transfers between devices: 21.2 us -> none  [body(): lax.all_gather(tokens, 'tp', axis=0, tiled=True)]
  transfers between devices with their start and end apart: 6 -> 6, of which waited for: 3 -> 3; matrix products, arithmetic and copies ran while one was open for 31% -> 32% of each run, Pallas kernels for 0% -> 0%
where the time goes in v1:
time: 458 us; the launch traced here: 453 us
  waiting for transfers between devices  127 us (28%)
  blocking collectives  126 us (28%)
  local copies, waits for them, and re-layouts  108 us (24%)
  other arithmetic  31.1 us (7%)
  matrix products  28.9 us (6%)
  starting transfers between devices  16.8 us (4%)
  between operations  15 us (3%)
    all_gather x1, waiting for transfers between devices, sent_together(): lax.all_gather(both, axis, axis=dim, tiled=True)  98.5 us
    all_gather x4, blocking collectives, all_in_one(): both, at, found = (lax.all_gather(jnp.concatenate(lines), axis), 0, {})  84.4 us
    all_to_all x1, blocking collectives, sum_at_owner(): lax.all_to_all(pieces, axis, split_axis=0, concat_axis=0, tiled=True)  41.7 us
    convert_element_type x40, local copies, waits for them, and re-layouts, prefix_by_axis(): part[k].astype(own.dtype)  38.4 us
    all_to_all x1, waiting for transfers between devices, body(): lax.all_to_all(jnp.stack([tokens] * lax.axis_size('tp')), 'tp', 0, 0)  26.1 us
    mul x16, local copies, waits for them, and re-layouts, combine_branches(): latter[0][:, None, None] * earlier[1] + latter[1]  19.9 us
    dot_general x5, matrix products, body(): jnp.dot(normed, weight, preferred_element_type=jnp.float32)  12.5 us
    reshape x6, local copies, waits for them, and re-layouts, split_heads(): return matrix.astype(jnp.float32).reshape(blocks, BLOCK, local_heads, HD)  9.85 us
  transfers between devices with their start and end apart: 6, of which 3 were waited for; matrix products, arithmetic and copies ran while one was open for 32% of the time, Pallas kernels for 0%

profile of v1, /device:TPU:32, one launch (start us, length us, event | category | flops | bytes accessed | tf_op | source)
XLA Modules:
  0.0 452.7 jit_solution(3704460201258676728)
XLA Ops:
  11.4 3.0 stack.6
  14.4 4.4 all-to-all-start
  19.8 1.8 reduce-window.6
  31.2 26.1 %all-to-all-done = bf16[8,96,2048]{2,1,0:T(8,128)(2,1)S(1)} async-done(((bf16[8,96,2048]{2,1,0:T(8,128)(2,1)}), bf16[8,96,2048]{2,1,0:T(8,128)(2,1)S(1)}, u32[]{:S(2)}, u32[]{:S(2)}) %all-to-all-start) | async-done | bytes 3145760 | tf_op jit(solution)/shard_map/all_to_all | solution.py:203
  58.1 2.6 fusion.1
  60.7 98.5 %all-gather.11.cloned.1.call-done = bf16[2048,768]{1,0:T(8,128)(2,1)} async-done(((bf16[32,768]{1,0:T(8,128)(2,1)}), bf16[2048,768]{1,0:T(8,128)(2,1)}) %all-gather.11.cloned.1.call-update) | async-done | bytes 3145744 | tf_op jit(solution)/shard_map/all_gather | solution.py:21
  159.2 3.0 convolution_convert_fusion.3
  164.4 2.8 fusion.28
  167.2 1.9 copy.305
  169.1 2.0 reshape.1754
  171.2 2.0 broadcast_multiply_fusion.2
  178.2 1.5 copy.318
  181.9 1.5 copy.350
  183.5 1.5 copy.349
  186.6 12.0 %all-gather.4 = bf16[4,129,64]{1,2,0:T(8,128)(2,1)S(1)} all-gather(bf16[1,129,64]{1,2,0:T(8,128)(2,1)S(1)} %get-tuple-element.78), channel_id=2, replica_groups=mesh['sp_0'=16,'sp_1'=4,'tp'=8] {'sp_1'}, dimensions={0}, use_global_device_ids=true | all-gather | bytes 82560 | tf_op jit(solution)/shard_map/all_gather | solution.py:69
  200.6 12.0 %all-gather.6 = bf16[4,129,64]{1,2,0:T(8,128)(2,1)S(1)} all-gather(bf16[1,129,64]{1,2,0:T(8,128)(2,1)S(1)} %get-tuple-element.79), channel_id=4, replica_groups=mesh['sp_0'=16,'sp_1'=4,'tp'=8] {'sp_1'}, dimensions={0}, use_global_device_ids=true | all-gather | bytes 82560 | tf_op jit(solution)/shard_map/all_gather | solution.py:69
  228.3 29.0 %all-gather.7 = bf16[16,129,64]{1,2,0:T(8,128)(2,1)S(1)} all-gather(bf16[1,129,64]{1,2,0:T(8,128)(2,1)S(1)} %maximum_bitcast_fusion.1), channel_id=5, replica_groups=mesh['sp_0'=16,'sp_1'=4,'tp'=8] {'sp_0'}, dimensions={0}, use_global_device_ids=true | all-gather | bytes 280704 | tf_op jit(solution)/shard_map/all_gather | solution.py:69
  275.3 31.4 %all-gather.5 = bf16[16,129,64]{1,2,0:T(8,128)(2,1)S(1)} all-gather(bf16[1,129,64]{1,2,0:T(8,128)(2,1)S(1)} %maximum_bitcast_fusion), channel_id=3, replica_groups=mesh['sp_0'=16,'sp_1'=4,'tp'=8] {'sp_0'}, dimensions={0}, use_global_device_ids=true | all-gather | bytes 280704 | tf_op jit(solution)/shard_map/all_gather | solution.py:69
  310.7 2.7 convolution_convert_fusion.2
  313.4 1.9 reshape.1862
  315.3 1.9 copy.306
  329.0 2.0 fusion.40
  331.0 2.0 fusion.26
  333.9 1.9 collective-permute-start
  335.8 6.2 %collective-permute-start.1 = (bf16[15,128]{1,0:T(8,128)(2,1)}, bf16[15,128]{1,0:T(8,128)(2,1)}, u32[]{:S(2)}, u32[]{:S(2)}) collective-permute-start(bf16[15,128]{1,0:T(8,128)(2,1)} %get-tuple-element.69), channel_id=1, source_target_pairs={{8,0},{16,8},{24,16},{32,24},{40,32},{48,40},{56,48},{64,56},{72,6... | collective-permute-start | bytes 11528 | tf_op jit(solution)/shard_map/ppermute | solution.py:32
  376.5 1.5 fusion.159
  378.7 4.2 all-to-all-start.1
  385.7 2.7 all-to-all-done.1
  388.5 4.7 %fusion.37 = f32[768,2048]{1,0:T(8,128)} fusion(bf16[2048,256]{1,0:T(8,128)(2,1)} %all-gather.13.cloned.1.call-done, f32[768,128]{1,0:T(8,128)S(1)} %get-tuple-element.26, f32[128]{0:T(128)S(1)} %copy-done.37, f32[768]{0:T(1024)S(1)} %get-tuple-element.112, f32[768]{0:T(1024)S(1)} %get-tuple-element.111), kind=kOutput, calls=%fused_computation.40 | convolution fusion | flops 403439616 | bytes 7215616 | tf_op jit(solution)/shard_map/dot_general | solution.py:287
  393.2 7.7 %add_convert_fusion = bf16[768,2048]{1,0:T(8,128)(2,1)S(1)} fusion(f32[768,2048]{1,0:T(8,128)} %fusion.37, bf16[2048,256]{1,0:T(8,128)(2,1)} %all-gather.13.cloned.1.call-done, bf16[768,2048]{1,0:T(8,128)(2,1)} %fusion.1, bf16[2048,768]{1,0:T(8,128)(2,1)} %all-gather.11.cloned.1.call-done, f32[768,128]{1,0:T(8,128)S(1)} %copy.379, ...), kind=kOutput, calls=%fused_computation.3 | convolution fusion | flops 809533440 | bytes 14811648 | tf_op jit(solution)/shard_map/dot_general | solution.py:289
  400.9 41.7 %all_to_all.16 = bf16[8,96,2048]{2,1,0:T(8,128)(2,1)} all-to-all(bf16[8,96,2048]{2,1,0:T(8,128)(2,1)S(1)} %bitcast.528), channel_id=1, replica_groups=mesh['sp_0'=16,'sp_1'=4,'tp'=8] {'tp'}, dimensions={0} | all-to-all | bytes 6291456 | tf_op jit(solution)/shard_map/all_to_all | solution.py:119
  442.6 3.3 reduce_sum.72
  (326 shorter events, 116.2 us)
Async XLA Ops:
  6.5 152.7 %all-gather.11.cloned.1.call-start = ((), (), s32[]{:S(2)}) async-start(), calls=%async_computation.3 | async-start | bytes 3194880 | tf_op jit(solution)/shard_map/all_gather | solution.py:21
  14.4 42.8 %all-to-all-start = ((bf16[8,96,2048]{2,1,0:T(8,128)(2,1)}), bf16[8,96,2048]{2,1,0:T(8,128)(2,1)S(1)}, u32[]{:S(2)}, u32[]{:S(2)}) async-start(bf16[8,96,2048]{2,1,0:T(8,128)(2,1)} %stack.6), calls=%async_computation | async-start | bytes 6291456 | tf_op jit(solution)/shard_map/all_to_all | solution.py:203
  18.9 39.2 %copy-start.26 = (f32[2048]{0:T(1024)S(1)}, f32[2048]{0:T(1024)}, u32[]{:S(2)}) copy-start(f32[2048]{0:T(1024)} %param.16) | copy-start | bytes 24580
  18.9 369.6 %all-gather.13.cloned.1.call-start = ((), (), s32[]{:S(2)}) async-start(), calls=%async_computation.4 | async-start | bytes 1064960 | tf_op jit(solution)/shard_map/all_gather | solution.py:103
  22.5 38.2 %copy-start.34 = (f32[2]{0:T(128)}, f32[2]{0:T(128)S(1)}, u32[]{:S(2)}) copy-start(f32[2]{0:T(128)S(1)} %get-tuple-element.7) | copy-start | bytes 28
  22.5 38.2 %copy-start.35 = (f32[2]{0:T(128)}, f32[2]{0:T(128)S(1)}, u32[]{:S(2)}) copy-start(f32[2]{0:T(128)S(1)} %get-tuple-element.8) | copy-start | bytes 28
  60.6 103.7 %copy-start = (bf16[768,2048]{1,0:T(8,128)(2,1)S(1)}, bf16[768,2048]{1,0:T(8,128)(2,1)}, u32[]{:S(2)}) copy-start(bf16[768,2048]{1,0:T(8,128)(2,1)} %fusion.1) | copy-start | bytes 9437188
  198.7 59.3 %copy-start.20 = (bf16[4,64]{1,0:T(4,128)(2,1)}, bf16[4,64]{1,0:T(4,128)(2,1)S(1)}, u32[]{:S(2)}) copy-start(bf16[4,64]{1,0:T(4,128)(2,1)S(1)} %slice_reduce_fusion.1) | copy-start | bytes 1540
  212.7 94.8 %copy-start.22 = (bf16[4,64]{1,0:T(4,128)(2,1)}, bf16[4,64]{1,0:T(4,128)(2,1)S(1)}, u32[]{:S(2)}) copy-start(bf16[4,64]{1,0:T(4,128)(2,1)S(1)} %slice_reduce_fusion) | copy-start | bytes 1540
  333.1 35.7 %copy-start.23 = (bf16[4,64]{1,0:T(4,128)(2,1)S(1)}, bf16[4,64]{1,0:T(4,128)(2,1)}, u32[]{:S(2)}) copy-start(bf16[4,64]{1,0:T(4,128)(2,1)} %copy-done.22) | copy-start | bytes 1540
  333.1 35.7 %copy-start.46 = (f32[2]{0:T(128)S(1)}, f32[2]{0:T(128)}, u32[]{:S(2)}) copy-start(f32[2]{0:T(128)} %get-tuple-element.23) | copy-start | bytes 28
  333.1 35.8 %copy-start.21 = (bf16[4,64]{1,0:T(4,128)(2,1)S(1)}, bf16[4,64]{1,0:T(4,128)(2,1)}, u32[]{:S(2)}) copy-start(bf16[4,64]{1,0:T(4,128)(2,1)} %copy-done.20) | copy-start | bytes 1540
  333.1 35.8 %copy-start.45 = (f32[2]{0:T(128)S(1)}, f32[2]{0:T(128)}, u32[]{:S(2)}) copy-start(f32[2]{0:T(128)} %get-tuple-element.15) | copy-start | bytes 28
  333.1 35.8 %copy-start.10 = (f32[1,128,64]{2,1,0:T(8,128)S(1)}, f32[1,128,64]{2,1,0:T(8,128)}, u32[]{:S(2)}) copy-start(f32[1,128,64]{2,1,0:T(8,128)} %copy.339) | copy-start | bytes 98308
  333.1 35.8 %copy-start.11 = (f32[1,128,64]{2,1,0:T(8,128)S(1)}, f32[1,128,64]{2,1,0:T(8,128)}, u32[]{:S(2)}) copy-start(f32[1,128,64]{2,1,0:T(8,128)} %copy.341) | copy-start | bytes 98308
  333.1 35.8 %copy-start.12 = (f32[1,128,64]{2,1,0:T(8,128)S(1)}, f32[1,128,64]{2,1,0:T(8,128)}, u32[]{:S(2)}) copy-start(f32[1,128,64]{2,1,0:T(8,128)} %copy.340) | copy-start | bytes 98308
  333.1 35.8 %copy-start.13 = (f32[1,128,64]{2,1,0:T(8,128)S(1)}, f32[1,128,64]{2,1,0:T(8,128)}, u32[]{:S(2)}) copy-start(f32[1,128,64]{2,1,0:T(8,128)} %copy.342) | copy-start | bytes 98308
  333.2 35.8 %copy-start.32 = (f32[2]{0:T(128)S(1)}, f32[2]{0:T(128)}, u32[]{:S(2)}) copy-start(f32[2]{0:T(128)} %copy-done.31) | copy-start | bytes 28
  333.2 35.8 %copy-start.36 = (f32[2]{0:T(128)S(1)}, f32[2]{0:T(128)}, u32[]{:S(2)}) copy-start(f32[2]{0:T(128)} %copy-done.35) | copy-start | bytes 28
  333.2 35.8 %copy-start.38 = (f32[2]{0:T(128)S(1)}, f32[2]{0:T(128)}, u32[]{:S(2)}) copy-start(f32[2]{0:T(128)} %get-tuple-element.147) | copy-start | bytes 28
  333.2 35.8 %copy-start.39 = (f32[2]{0:T(128)S(1)}, f32[2]{0:T(128)}, u32[]{:S(2)}) copy-start(f32[2]{0:T(128)} %get-tuple-element.114) | copy-start | bytes 28
  333.2 35.8 %copy-start.40 = (f32[2]{0:T(128)S(1)}, f32[2]{0:T(128)}, u32[]{:S(2)}) copy-start(f32[2]{0:T(128)} %get-tuple-element.115) | copy-start | bytes 28
  333.2 35.8 %copy-start.41 = (f32[2]{0:T(128)S(1)}, f32[2]{0:T(128)}, u32[]{:S(2)}) copy-start(f32[2]{0:T(128)} %get-tuple-element.116) | copy-start | bytes 28
  333.2 35.8 %copy-start.42 = (f32[2]{0:T(128)S(1)}, f32[2]{0:T(128)}, u32[]{:S(2)}) copy-start(f32[2]{0:T(128)} %get-tuple-element.117) | copy-start | bytes 28
  333.2 35.8 %copy-start.43 = (f32[2]{0:T(128)S(1)}, f32[2]{0:T(128)}, u32[]{:S(2)}) copy-start(f32[2]{0:T(128)} %get-tuple-element.118) | copy-start | bytes 28
  333.2 37.0 %copy-start.6 = (f32[1,128,64]{2,1,0:T(8,128)S(1)}, f32[1,128,64]{2,1,0:T(8,128)}, u32[]{:S(2)}) copy-start(f32[1,128,64]{2,1,0:T(8,128)} %copy.370) | copy-start | bytes 98308
  333.2 37.0 %copy-start.7 = (f32[1,128,64]{2,1,0:T(8,128)S(1)}, f32[1,128,64]{2,1,0:T(8,128)}, u32[]{:S(2)}) copy-start(f32[1,128,64]{2,1,0:T(8,128)} %copy.372) | copy-start | bytes 98308
  333.3 37.0 %copy-start.8 = (f32[1,128,64]{2,1,0:T(8,128)S(1)}, f32[1,128,64]{2,1,0:T(8,128)}, u32[]{:S(2)}) copy-start(f32[1,128,64]{2,1,0:T(8,128)} %copy.371) | copy-start | bytes 98308
  333.3 37.0 %copy-start.9 = (f32[1,128,64]{2,1,0:T(8,128)S(1)}, f32[1,128,64]{2,1,0:T(8,128)}, u32[]{:S(2)}) copy-start(f32[1,128,64]{2,1,0:T(8,128)} %copy.373) | copy-start | bytes 98308
  333.9 41.5 %collective-permute-start = (bf16[15,128]{1,0:T(8,128)(2,1)}, bf16[15,128]{1,0:T(8,128)(2,1)}, u32[]{:S(2)}, u32[]{:S(2)}) collective-permute-start(bf16[15,128]{1,0:T(8,128)(2,1)} %get-tuple-element.68), channel_id=1, source_target_pairs={{0,8},{8,16},{16,24},{24,32},{32,40},{40,48},{48,56},{56,64},{64,7... | collective-permute-start | bytes 11528 | tf_op jit(solution)/shard_map/ppermute | solution.py:31
  335.8 39.6 %collective-permute-start.1 = (bf16[15,128]{1,0:T(8,128)(2,1)}, bf16[15,128]{1,0:T(8,128)(2,1)}, u32[]{:S(2)}, u32[]{:S(2)}) collective-permute-start(bf16[15,128]{1,0:T(8,128)(2,1)} %get-tuple-element.69), channel_id=1, source_target_pairs={{8,0},{16,8},{24,16},{32,24},{40,32},{48,40},{56,48},{64,56},{72,6... | collective-permute-start | bytes 11528 | tf_op jit(solution)/shard_map/ppermute | solution.py:32
  378.7 9.7 %all-to-all-start.1 = ((f32[8,1,1536]{2,1,0:T(1,128)}), f32[8,1,1536]{2,1,0:T(1,128)S(1)}, u32[]{:S(2)}, u32[]{:S(2)}) async-start(f32[8,1,1536]{2,1,0:T(1,128)} %broadcast_in_dim.2), calls=%async_computation.1 | async-start | bytes 98304 | tf_op jit(solution)/shard_map/all_to_all | solution.py:39
  (53 other events, 345.0 us)
Sparse Core Ops, SparseCore 0:
  11.5 147.6 all-gather.10
  162.1 133.9 all-gather.12
